TPU v7x, 512 devices: a whole 4x4x16 slice. The times are simulated.
512 devices in a mesh: ep: 32 (over z, core), tp: 16 (over y, x).
Axes of the slice: x: 4, y: 4, z: 16, core: 2. Of those that a mesh axis runs over, the one named last changes fastest.
Arguments:
- conv_input: bfloat16 [1024, 65536], P('tp', 'ep'), may hold values from -6 to 6
- out_gate: bfloat16 [1024, 65536], P('tp', 'ep'), may hold values from -6 to 6
- in_gate: bfloat16 [1024, 65536], P('tp', 'ep'), may hold values from -6 to 6
- conv_taps: float32 [3, 1024], replicated, may hold values from -3.5 to 3.5
- mixer_proj: bfloat16 [1024, 2048], P(None, 'tp'), may hold values from -0.1875 to 0.1875
- token_rows: bfloat16 [8192, 2048], P('ep', 'tp'), may hold values from -4000 to 4000
- routes: int32 [8192, 2], P('ep'), may hold values from 0 to 31, as said below
- route_weights: float32 [8192, 2], P('ep'), may hold values from 0.3 to 1
- expert_gate: bfloat16 [32, 2048, 4096], P('ep', None, 'tp'), may hold values from -0.125 to 0.125
- expert_up: bfloat16 [32, 2048, 4096], P('ep', None, 'tp'), may hold values from -0.125 to 0.125
- expert_down: bfloat16 [32, 4096, 2048], P('ep', 'tp'), may hold values from -0.125 to 0.125
Outputs:
- mixed_out: bfloat16 [65536, 2048], P('ep', 'tp')
- expert_out: bfloat16 [8192, 2048], P('ep', 'tp')
Inputs may be any that keep to these rules, and one draw needn't show every extreme that they name: `routes`: in each aligned block of 256 rows, no expert is named more than 32 times and one expert, the same in every block, exactly 32 times; the two experts of a row differ.
All inputs are finite; a program needn't handle non-finite values.
Results may differ from a plain program's by a relative error of at most 0.015.
Values may be sent and summed in bfloat16 or wider, within the bound.
No kernel may reach another device: no remote copies, remote signals or barrier semaphores. Data moves between devices by JAX's collectives and lax.ppermute only.
A program may use at most 64 MiB of HBM per device.

v0:
```python
import jax
import jax.numpy as jnp
from jax import lax
from jax.sharding import PartitionSpec as P

KERNEL = 3


EPSILON = 1e-06


def passed_along(value, axis, by):
    devices = lax.axis_size(axis)
    pairs = [(i, i + by) for i in range(devices) if 0 <= i + by < devices]
    return lax.ppermute(value, axis, pairs)


def split_up(value, dim, devices):
    before, after = (value.shape[:dim], value.shape[dim + 1 :])
    return jnp.moveaxis(value.reshape(*before, devices, -1, *after), dim, 0)


def sent_and_summed(value, axis, dim):
    blocks = split_up(value, dim, lax.axis_size(axis))
    arrived = lax.all_to_all(blocks, axis, split_axis=0, concat_axis=0, tiled=True)
    return arrived.astype(jnp.float32).sum(axis=0)


def slot_places(route_ids, capacity, experts):
    flat_ids = route_ids.reshape(-1)
    hit_table = (flat_ids[:, None] == jnp.arange(experts, dtype=jnp.int32)[None, :]).astype(
        jnp.int32
    )
    earlier = jnp.cumsum(hit_table, axis=0) - hit_table
    slot_rank = jnp.sum(earlier * hit_table, axis=1)
    return flat_ids * capacity + slot_rank


def body(
    conv_input,
    out_gate,
    in_gate,
    conv_taps,
    mixer_proj,
    token_rows,
    routes,
    route_weights,
    expert_gate,
    expert_up,
    expert_down,
):
    width_part = conv_input.shape[0]
    length = conv_input.shape[1]
    offset = lax.axis_index("tp") * width_part
    local_taps = lax.dynamic_slice_in_dim(conv_taps, offset, width_part, 1)
    z_rows = (conv_input.astype(jnp.float32) * in_gate.astype(jnp.float32)).astype(jnp.bfloat16)
    rim_rows = passed_along(z_rows[:, length - (KERNEL - 1) :], "ep", 1)
    longer = jnp.concatenate([rim_rows, z_rows], axis=1).astype(jnp.float32)
    conv_sum = jnp.zeros(z_rows.shape, jnp.float32)
    for lag_index in range(KERNEL):
        begin = KERNEL - 1 - lag_index
        conv_sum = conv_sum + local_taps[lag_index][:, None] * longer[:, begin : begin + length]
    gated = (out_gate.astype(jnp.float32) * conv_sum).astype(jnp.bfloat16)
    mixed_sum = lax.dot_general(
        lax.all_gather(gated, "tp", axis=0, tiled=True),
        mixer_proj,
        (((0,), (0,)), ((), ())),
        preferred_element_type=jnp.float32,
    )
    mixed_out = mixed_sum.astype(jnp.bfloat16)
    experts = lax.axis_size("ep")
    rows_b = token_rows.shape[0]
    cols_part = token_rows.shape[1]
    capacity = 4 * rows_b // experts
    slot_total = experts * capacity
    places = slot_places(routes, capacity, experts)
    sources = jnp.arange(2 * rows_b, dtype=jnp.int32) // 2
    gate_weight = expert_gate[0]
    up_weight = expert_up[0]
    down_weight = expert_down[0]
    feature_count = cols_part * lax.axis_size("tp")
    buffer = jnp.zeros((slot_total, cols_part), jnp.bfloat16).at[places].set(token_rows[sources])
    arrived = lax.all_to_all(
        buffer.reshape(experts, capacity, cols_part), "ep", split_axis=0, concat_axis=0, tiled=True
    )
    arrived = arrived.reshape(slot_total, cols_part)
    part_in = lax.all_gather(arrived, "tp", axis=1, tiled=True)
    gate_sum = jnp.dot(part_in, gate_weight, preferred_element_type=jnp.float32)
    up_sum = jnp.dot(part_in, up_weight, preferred_element_type=jnp.float32)
    squares = jnp.sum(jnp.square(part_in.astype(jnp.float32)), axis=1)
    row_scale = lax.rsqrt(squares / feature_count + EPSILON)[:, None]
    hidden = (jax.nn.silu(row_scale * gate_sum) * (row_scale * up_sum)).astype(jnp.bfloat16)
    summed = sent_and_summed(
        lax.dot_general(
            down_weight, hidden, (((0,), (1,)), ((), ())), preferred_element_type=jnp.float32
        ).astype(jnp.bfloat16),
        "tp",
        0,
    )
    expert_rows = summed.astype(jnp.bfloat16).reshape(cols_part, experts, capacity)
    returned = lax.all_to_all(expert_rows, "ep", split_axis=1, concat_axis=1, tiled=True).reshape(
        cols_part, slot_total
    )
    picked = returned[:, places].astype(jnp.float32).reshape(cols_part, rows_b, 2)
    combined = jnp.sum(picked * route_weights[None, :, :], axis=2)
    expert_out = combined.T.astype(jnp.bfloat16)
    return (mixed_out, expert_out)


def solution(mesh):
    return jax.shard_map(
        body,
        mesh=mesh,
        in_specs=(
            P("tp", "ep"),
            P("tp", "ep"),
            P("tp", "ep"),
            P(),
            P(None, "tp"),
            P("ep", "tp"),
            P("ep", None),
            P("ep", None),
            P("ep", None, "tp"),
            P("ep", None, "tp"),
            P("ep", "tp", None),
        ),
        out_specs=(P("ep", "tp"), P("ep", "tp")),
        check_vma=False,
    )
```

profile of v0, /device:TPU:1, one launch (start us, length us, event | category | flops | bytes accessed | tf_op | source)
XLA Modules:
  0.0 242.8 jit_solution(143505425020026601)
XLA Ops:
  7.2 0.9 copy.26
  8.4 0.7 broadcast_multiply_fusion
  9.1 1.2 reduce-window.6
  10.3 0.2 slice_reduce_fusion
  11.0 4.9 %scatter_custom_fusion = bf16[1024,128]{1,0:T(8,128)(2,1)S(1)} fusion(s32[512]{0:T(512)S(1)} %bitcast.65, bf16[256,128]{1,0:T(8,128)(2,1)} %param.16, s32[1024]{0:T(1024)S(1)} %pad_clamp_fusion.1, bf16[]{:T(256)} %constant.39.clone.1), kind=kCustom, calls=%fused_computation.26 | custom fusion | bytes 262656 | tf_op jit(solution)/shard_map/scatter | solution.py:82
  15.9 38.9 %all_to_all.15 = bf16[32,32,128]{2,1,0:T(8,128)(2,1)} all-to-all(bf16[32,32,128]{2,1,0:T(8,128)(2,1)S(1)} %bitcast.63), channel_id=1, replica_groups=mesh['ep'=32,'tp'=16] {'ep'}, dimensions={0} | all-to-all | bytes 524288 | tf_op jit(solution)/shard_map/all_to_all | solution.py:83
  54.9 1.2 multiply_convert_fusion
  56.1 2.2 collective-permute-start
  58.4 0.8 constant_dynamic-slice_fusion
  59.4 2.0 fusion.9
  61.4 55.6 %all-gather.5.cloned.1.call-done = bf16[1024,2048]{1,0:T(8,128)(2,1)} async-done(((bf16[1024,128]{1,0:T(8,128)(2,1)}), bf16[1024,2048]{1,0:T(8,128)(2,1)}) %all-gather.5.cloned.1.call-update) | async-done | bytes 4194320 | tf_op jit(solution)/shard_map/all_gather | solution.py:87
  117.1 3.2 %multiply_reduce_fusion = f32[1024]{0:T(1024)S(1)} fusion(bf16[1024,2048]{1,0:T(8,128)(2,1)} %all-gather.5.cloned.1.call-done), kind=kLoop, calls=%fused_computation.3 | loop fusion | flops 6290432 | bytes 4198400 | tf_op jit(solution)/shard_map/reduce_sum | solution.py:90
  120.3 0.2 copy-done.1
  120.5 2.3 convolution_multiply_fusion.1
  122.8 8.8 %convert_bitcast_fusion = bf16[128,16,8,128]{3,2,1,0:T(8,128)(2,1)} fusion(bf16[1,256,2048]{2,1,0:T(8,128)(2,1)S(1)} %copy-done, bf16[1024,2048]{1,0:T(8,128)(2,1)} %all-gather.5.cloned.1.call-done, bf16[1,2048,256]{2,1,0:T(8,128)(2,1)S(1)} %copy-done.4, f32[1024,256]{1,0:T(8,128)} %convolution_multiply_fusion.1, f32[1024]{0:T(1024)S(1)} %add_rsqrt_fusion), kind=kOutput, calls=%fused_computation.5 | convolution fusion | flops 2151415808 | bytes 11538432 | tf_op jit(solution)/shard_map/dot_general | solution.py:94
  131.6 3.3 %copy.35 = bf16[128,16,8,128]{3,2,0,1:T(8,128)(2,1)S(1)} copy(bf16[128,16,8,128]{3,2,1,0:T(8,128)(2,1)} %convert_bitcast_fusion) | data formatting | bytes 8388608 | tf_op jit(solution)/shard_map/reshape | solution.py:20
  134.9 58.8 %all_to_all.16 = bf16[16,128,1024]{1,2,0:T(8,128)(2,1)} all-to-all(bf16[16,128,1024]{1,2,0:T(8,128)(2,1)S(1)} %bitcast.59), channel_id=1, replica_groups=mesh['ep'=32,'tp'=16] {'tp'}, dimensions={0} | all-to-all | bytes 8388608 | tf_op jit(solution)/shard_map/all_to_all | solution.py:25
  193.7 3.9 %reduce_sum.44 = bf16[128,1024]{0,1:T(8,128)(2,1)} reduce(bf16[16,128,1024]{1,2,0:T(8,128)(2,1)} %all_to_all.16, bf16[]{:T(256)} %constant.39.clone.1), dimensions={0}, to_apply=%region_5.6 | reduce | flops 1966080 | bytes 4456450 | tf_op jit(solution)/shard_map/reduce_sum | solution.py:26
  197.6 13.7 %all-to-all-start.2 = ((bf16[128,32,32]{0,2,1:T(8,128)(2,1)}), bf16[128,32,32]{0,2,1:T(8,128)(2,1)S(1)}, u32[]{:S(2)}, u32[]{:S(2)}) async-start(bf16[128,32,32]{0,2,1:T(8,128)(2,1)} %bitcast.13), calls=%async_computation.2 | async-start | bytes 524288 | tf_op jit(solution)/shard_map/all_to_all | solution.py:101
  211.5 3.2 %all-gather.3.cloned.1.call-done = bf16[1024,2048]{1,0:T(8,128)(2,1)} async-done(((bf16[64,2048]{1,0:T(8,128)(2,1)}), bf16[1024,2048]{1,0:T(8,128)(2,1)}) %all-gather.3.cloned.1.call-update) | async-done | bytes 4194320 | tf_op jit(solution)/shard_map/all_gather | solution.py:65
  214.7 4.3 %convolution_convert_fusion = bf16[2048,128]{1,0:T(8,128)(2,1)} fusion(bf16[1024,2048]{1,0:T(8,128)(2,1)} %all-gather.3.cloned.1.call-done, bf16[1024,128]{1,0:T(8,128)(2,1)S(1)} %copy-done.5), kind=kOutput, calls=%fused_computation.6 | convolution fusion | flops 537133056 | bytes 4980736 | tf_op jit(solution)/shard_map/dot_general | solution.py:64
  219.0 14.6 %all-to-all-done.2 = bf16[128,32,32]{0,2,1:T(8,128)(2,1)S(1)} async-done(((bf16[128,32,32]{0,2,1:T(8,128)(2,1)}), bf16[128,32,32]{0,2,1:T(8,128)(2,1)S(1)}, u32[]{:S(2)}, u32[]{:S(2)}) %all-to-all-start.2) | async-done | bytes 262176 | tf_op jit(solution)/shard_map/all_to_all | solution.py:101
  233.6 1.3 gather_fusion
  234.9 1.0 multiply_reduce_fusion.1
  (34 shorter events, 1.4 us)
Async XLA Ops:
  7.2 115.7 %copy-start = (bf16[1,256,2048]{2,1,0:T(8,128)(2,1)S(1)}, bf16[1,256,2048]{2,1,0:T(8,128)(2,1)}, u32[]{:S(2)}) copy-start(bf16[1,256,2048]{2,1,0:T(8,128)(2,1)} %param.21) | copy-start | bytes 3145732
  7.2 109.9 %all-gather.5.cloned.1.call-start = ((), (), s32[]{:S(2)}) async-start(), calls=%async_computation.4 | async-start | bytes 4456448 | tf_op jit(solution)/shard_map/all_gather | solution.py:87
  54.8 65.5 %copy-start.3 = (bf16[1,2048,256]{2,1,0:T(8,128)(2,1)S(1)}, bf16[1,2048,256]{2,1,0:T(8,128)(2,1)}, u32[]{:S(2)}) copy-start(bf16[1,2048,256]{2,1,0:T(8,128)(2,1)} %param.19) | copy-start | bytes 3145732
  54.8 159.8 %all-gather.3.cloned.1.call-start = ((), (), s32[]{:S(2)}) async-start(), calls=%async_computation.3 | async-start | bytes 4456448 | tf_op jit(solution)/shard_map/all_gather | solution.py:65
  56.1 3.1 %collective-permute-start = (bf16[64,2]{1,0:T(8,128)(2,1)S(1)}, bf16[64,2]{1,0:T(8,128)(2,1)S(1)}, u32[]{:S(2)}, u32[]{:S(2)}) collective-permute-start(bf16[64,2]{1,0:T(8,128)(2,1)S(1)} %slice.40), channel_id=1, source_target_pairs={{0,16},{16,32},{32,48},{48,64},{64,80},{80,96},{96,112},{112,128},... | collective-permute-start | bytes 776 | tf_op jit(solution)/shard_map/ppermute | solution.py:15
  117.1 3.4 %copy-start.1 = (bf16[1024,2048]{1,0:T(8,128)(2,1)S(1)}, bf16[1024,2048]{1,0:T(8,128)(2,1)}, u32[]{:S(2)}) copy-start(bf16[1024,2048]{1,0:T(8,128)(2,1)} %all-gather.5.cloned.1.call-done) | copy-start | bytes 12582916
  120.3 2.5 %copy-start.4 = (bf16[1,2048,256]{2,1,0:T(8,128)(2,1)S(1)}, bf16[1,2048,256]{2,1,0:T(8,128)(2,1)}, u32[]{:S(2)}) copy-start(bf16[1,2048,256]{2,1,0:T(8,128)(2,1)} %param.20) | copy-start | bytes 3145732
  193.7 17.6 %copy-start.2 = (f32[256,2]{0,1:T(2,128)S(1)}, f32[256,2]{0,1:T(2,128)}, u32[]{:S(2)}) copy-start(f32[256,2]{0,1:T(2,128)} %param.18) | copy-start | bytes 6148
  193.7 21.0 %copy-start.5 = (bf16[1024,128]{1,0:T(8,128)(2,1)S(1)}, bf16[1024,128]{1,0:T(8,128)(2,1)}, u32[]{:S(2)}) copy-start(bf16[1024,128]{1,0:T(8,128)(2,1)} %param.15) | copy-start | bytes 786436
  197.6 35.9 %all-to-all-start.2 = ((bf16[128,32,32]{0,2,1:T(8,128)(2,1)}), bf16[128,32,32]{0,2,1:T(8,128)(2,1)S(1)}, u32[]{:S(2)}, u32[]{:S(2)}) async-start(bf16[128,32,32]{0,2,1:T(8,128)(2,1)} %bitcast.13), calls=%async_computation.2 | async-start | bytes 524288 | tf_op jit(solution)/shard_map/all_to_all | solution.py:101
Sparse Core Ops, SparseCore 0:
  54.9 62.0 all-gather.4
  120.6 93.9 all-gather.2
where the time goes:
time: 243 us
  blocking collectives  97.7 us (40%)
  waiting for transfers between devices  73.6 us (30%)
  starting transfers between devices  16 us (7%)
  matrix products  15.4 us (6%)
  between operations  14.2 us (6%)
  other arithmetic  13.6 us (6%)
  local copies, waits for them, and re-layouts  12.4 us (5%)
    all_to_all x1, blocking collectives, sent_and_summed(): lax.all_to_all(blocks, axis, split_axis=0, concat_axis=0, tiled=True)  58.8 us
    all_gather x1, waiting for transfers between devices, body(): part_in = lax.all_gather(arrived, 'tp', axis=1, tiled=True)  55.6 us
    all_to_all x1, blocking collectives, body(): lax.all_to_all(buffer.reshape(experts, capacity, cols_part), 'ep', split_...  38.9 us
    all_to_all x1, waiting for transfers between devices, body(): lax.all_to_all(expert_rows, 'ep', split_axis=1, concat_axis=1, tiled=True)  14.6 us
    all_to_all x1, starting transfers between devices, body(): lax.all_to_all(expert_rows, 'ep', split_axis=1, concat_axis=1, tiled=True)  13.7 us
    dot_general x1, matrix products, body(): lax.dot_general(down_weight, hidden, (((0,), (1,)), ((), ())), preferred_...  8.82 us
    scatter x1, local copies, waits for them, and re-layouts, body(): jnp.zeros((slot_total, cols_part), jnp.bfloat16).at[places]  4.9 us
  transfers between devices with their start and end apart: 4, of which 4 were waited for; matrix products, arithmetic and copies ran while one was open for 12% of the time, Pallas kernels for 0%

commit v1 on v0

v1 whole, which is shorter than its diff:
```python
import jax
import jax.numpy as jnp
from jax import lax
from jax.experimental import pallas as pl
from jax.experimental.pallas import tpu as pltpu
from jax.sharding import Mesh
from jax.sharding import PartitionSpec as P

KERNEL = 3
EPSILON = 1e-06
BF = jnp.bfloat16
F32 = jnp.float32


def expert_kernel(x_ref, gate_ref, up_ref, down_ref, out_ref):
    parts = x_ref.shape[0]
    cols = x_ref.shape[2]
    x = jnp.concatenate([x_ref[j] for j in range(parts)], axis=1)
    values = x.astype(F32)
    squares = jnp.sum(values * values, axis=1, keepdims=True)
    scale = lax.rsqrt(squares / (parts * cols) + EPSILON)
    gate = scale * jnp.dot(x, gate_ref[...], preferred_element_type=F32)
    up = scale * jnp.dot(x, up_ref[...], preferred_element_type=F32)
    hidden = (jax.nn.silu(gate) * up).astype(BF)
    part = jnp.dot(hidden, down_ref[...], preferred_element_type=F32).astype(BF)
    for j in range(parts):
        out_ref[j] = part[:, j * cols : (j + 1) * cols]


def expert_part(x, gate_weight, up_weight, down_weight, tile):
    parts, rows, cols = x.shape
    whole = lambda w: pl.BlockSpec(w.shape, lambda i: (0, 0))
    return pl.pallas_call(
        expert_kernel,
        grid=(rows // tile,),
        in_specs=[
            pl.BlockSpec((parts, tile, cols), lambda i: (0, i, 0)),
            whole(gate_weight),
            whole(up_weight),
            whole(down_weight),
        ],
        out_specs=pl.BlockSpec((parts, tile, cols), lambda i: (0, i, 0)),
        out_shape=jax.ShapeDtypeStruct(x.shape, BF),
        compiler_params=pltpu.CompilerParams(vmem_limit_bytes=40 * 1024 * 1024),
        cost_estimate=pl.CostEstimate(
            flops=6 * rows * parts * cols * gate_weight.shape[1],
            bytes_accessed=2 * 2 * rows * parts * cols + 6 * gate_weight.size,
            transcendentals=rows * gate_weight.shape[1],
        ),
    )(x, gate_weight, up_weight, down_weight)


def sum_parts(arrived):
    return arrived.astype(F32).sum(axis=0).astype(BF)


def body(
    conv_input,
    out_gate,
    in_gate,
    conv_taps,
    mixer_proj,
    token_rows,
    routes,
    route_weights,
    expert_gate,
    expert_up,
    expert_down,
):
    depth = lax.axis_size("z")
    experts = 2 * depth
    tp = lax.axis_size("tp")
    core = lax.axis_index("c")
    rows_b, cols_part = token_rows.shape
    capacity = 4 * rows_b // experts
    slot_total = experts * capacity
    half = slot_total // 2

    expert_ids = jnp.arange(experts, dtype=jnp.int32)[None, :]
    hit0 = routes[:, 0:1] == expert_ids
    hit1 = routes[:, 1:2] == expert_ids
    hits = (hit0 | hit1).astype(BF)
    order = jnp.arange(rows_b, dtype=jnp.int32)
    earlier_rows = (order[None, :] < order[:, None]).astype(BF)
    earlier = jnp.dot(earlier_rows, hits, preferred_element_type=F32).astype(jnp.int32)
    places = []
    for k, hit in enumerate((hit0, hit1)):
        slot = jnp.sum(jnp.where(hit, earlier, 0), axis=1)
        places.append((routes[:, k] ^ core) * capacity + slot)
    slot_ids = jnp.arange(slot_total, dtype=jnp.int32)[None, :]
    pick0 = places[0][:, None] == slot_ids
    pick1 = places[1][:, None] == slot_ids
    pick_any = (pick0 | pick1).astype(BF)
    outgoing = lax.dot_general(
        pick_any, token_rows, (((0,), (0,)), ((), ())), preferred_element_type=F32
    ).astype(BF)

    length = conv_input.shape[1]
    width_part = conv_input.shape[0]
    offset = lax.axis_index("tp") * width_part
    local_taps = lax.dynamic_slice_in_dim(conv_taps, offset, width_part, 1)
    rim_from = length - (KERNEL - 1)
    rim = (
        conv_input[:, rim_from:].astype(F32) * in_gate[:, rim_from:].astype(F32)
    ).astype(BF)
    pairs = [(i, i + 1) for i in range(experts - 1)]
    rim = lax.ppermute(rim, ("z", "c"), pairs)
    z_rows = (conv_input.astype(F32) * in_gate.astype(F32)).astype(BF)
    longer = jnp.concatenate([rim, z_rows], axis=1).astype(F32)
    conv_sum = jnp.zeros(z_rows.shape, F32)
    for lag in range(KERNEL):
        begin = KERNEL - 1 - lag
        conv_sum = conv_sum + local_taps[lag][:, None] * longer[:, begin : begin + length]
    gated = (out_gate.astype(F32) * conv_sum).astype(BF)
    first = gated[:, : length // 2]
    y_first = lax.all_gather(first, "tp", axis=0, tiled=True)

    swap = [(0, 1), (1, 0)]
    arrived = lax.all_to_all(
        outgoing.reshape(depth, 2, capacity, cols_part), "z", 0, 0, tiled=True
    )
    arrived, gated = lax.optimization_barrier((arrived, gated))
    rows_own = arrived[:, 0].reshape(half, cols_part)
    rows_other = lax.ppermute(arrived[:, 1].reshape(half, cols_part), "c", swap)

    x_own = lax.all_gather(rows_own, "tp", axis=0, tiled=False)
    x_other = lax.all_to_all(
        jnp.broadcast_to(rows_other[None], (tp, half, cols_part)), "tp", 0, 0, tiled=True
    )
    second, x_other = lax.optimization_barrier((gated[:, length // 2 :], x_other))
    y_second = lax.all_gather(second, "tp", axis=0, tiled=True)

    weights = (expert_gate[0], expert_up[0], expert_down[0])
    tile = half // 2
    part_other = expert_part(x_other, *weights, tile)
    sums_other = lax.all_to_all(part_other, "tp", 0, 0, tiled=True)
    part_own = expert_part(x_own, *weights, tile)
    part_own, sums_other = lax.optimization_barrier((part_own, sums_other))
    sums_own = lax.all_to_all(part_own, "tp", 0, 0, tiled=True)
    back_other = lax.ppermute(sum_parts(sums_other), "c", swap)
    back_own = sum_parts(sums_own)
    back = jnp.stack(
        [
            back_own.reshape(depth, capacity, cols_part),
            back_other.reshape(depth, capacity, cols_part),
        ],
        axis=1,
    )
    returned = lax.all_to_all(back, "z", 0, 0, tiled=True).reshape(slot_total, cols_part)
    picked0 = jnp.dot(pick0.astype(BF), returned, preferred_element_type=F32)
    picked1 = jnp.dot(pick1.astype(BF), returned, preferred_element_type=F32)
    expert_out = (
        picked0 * route_weights[:, 0:1] + picked1 * route_weights[:, 1:2]
    ).astype(BF)

    mixed = [
        lax.dot_general(
            y, mixer_proj, (((0,), (0,)), ((), ())), preferred_element_type=F32
        ).astype(BF)
        for y in (y_first, y_second)
    ]
    mixed_out = jnp.concatenate(mixed, axis=0)
    return (mixed_out, expert_out)


def solution(mesh):
    ep, tp = mesh.devices.shape
    fine = Mesh(mesh.devices.reshape(ep // 2, 2, tp), ("z", "c", "tp"))
    both = ("z", "c")
    return jax.shard_map(
        body,
        mesh=fine,
        in_specs=(
            P("tp", both),
            P("tp", both),
            P("tp", both),
            P(),
            P(None, "tp"),
            P(both, "tp"),
            P(both, None),
            P(both, None),
            P(both, None, "tp"),
            P(both, None, "tp"),
            P(both, "tp", None),
        ),
        out_specs=(P(both, "tp"), P(both, "tp")),
        check_vma=False,
    )
```

time: 243 us -> 286 us (1.18)
  waiting for transfers between devices: 73.6 us -> 186 us
  blocking collectives: 97.7 us -> 0 us
  starting transfers between devices: 16 us -> 51 us
  other arithmetic: 13.6 us -> 6.13 us
  matrix products: 15.4 us -> 8.36 us
  Pallas kernels: 0 us -> 6.65 us
    all_to_all x2 -> x0, blocking collectives: 97.7 us -> none  [the longest x1 58.8 us: sent_and_summed(): lax.all_to_all(blocks, axis, split_axis=0, concat_axis=0, tiled=True)]
    all_to_all x1 -> x5, waiting for transfers between devices: 14.6 us -> 84.4 us  [the longest x1 33.5 us: body(): lax.all_to_all(jnp.broadcast_to(rows_other[None], (tp, half, cols_part)),...]
    all_gather x2 -> x3, waiting for transfers between devices: 58.8 us -> 100 us  [the longest x1 60.4 us: body(): y_second = lax.all_gather(second, 'tp', axis=0, tiled=True)]
    all_to_all x1 -> x5, starting transfers between devices: 13.7 us -> 39.4 us  [the longest x1 14 us: body(): lax.all_to_all(outgoing.reshape(depth, 2, capacity, cols_part), 'z', 0, 0...]
    ppermute x1 -> x3, starting transfers between devices: 2.23 us -> 11.5 us  [the longest x1 4.92 us: body(): rim = lax.ppermute(rim, ('z', 'c'), pairs)]
    dot_general x3 -> x6, matrix products: 15.4 us -> 8.36 us  [the longest x2 4.69 us: body(): lax.dot_general(y, mixer_proj, (((0,), (0,)), ((), ())), preferred_elemen...]
    pallas_call x0 -> x2, Pallas kernels: none -> 6.65 us  [expert_part(): pl.pallas_call(expert_kernel, grid=(rows // tile,), in_specs=[pl.BlockSpe...]
    reduce_sum x4 -> x2, other arithmetic: 8.3 us -> 2.18 us  [sum_parts(): return arrived.astype(F32).sum(axis=0).astype(BF)]
  transfers between devices with their start and end apart: 4 -> 11, of which waited for: 4 -> 8; matrix products, arithmetic and copies ran while one was open for 12% -> 7% of each run, Pallas kernels for 0% -> 2%
where the time goes in v1:
time: 286 us; the launch traced here: 284 us
  waiting for transfers between devices  186 us (65%)
  starting transfers between devices  51 us (18%)
  between operations  13.9 us (5%)
  local copies, waits for them, and re-layouts  12.2 us (4%)
  matrix products  8.36 us (3%)
  Pallas kernels  6.65 us (2%)
  other arithmetic  6.13 us (2%)
    all_gather x1, waiting for transfers between devices, body(): y_second = lax.all_gather(second, 'tp', axis=0, tiled=True)  60.4 us
    all_to_all x1, waiting for transfers between devices, body(): lax.all_to_all(jnp.broadcast_to(rows_other[None], (tp, half, cols_part)),...  33.5 us
    all_to_all x1, waiting for transfers between devices, body(): sums_own = lax.all_to_all(part_own, 'tp', 0, 0, tiled=True)  28.1 us
    all_gather x1, waiting for transfers between devices, body(): x_own = lax.all_gather(rows_own, 'tp', axis=0, tiled=False)  23.7 us
    all_gather x1, waiting for transfers between devices, body(): y_first = lax.all_gather(first, 'tp', axis=0, tiled=True)  16 us
    all_to_all x1, waiting for transfers between devices, body(): lax.all_to_all(outgoing.reshape(depth, 2, capacity, cols_part), 'z', 0, 0...  14.3 us
    all_to_all x1, starting transfers between devices, body(): lax.all_to_all(outgoing.reshape(depth, 2, capacity, cols_part), 'z', 0, 0...  14 us
    all_to_all x1, starting transfers between devices, body(): lax.all_to_all(back, 'z', 0, 0, tiled=True).reshape(slot_total, cols_part)  10.1 us
  transfers between devices with their start and end apart: 11, of which 8 were waited for; matrix products, arithmetic and copies ran while one was open for 7% of the time, Pallas kernels for 2%

profile of v1, /device:TPU:1, one launch (start us, length us, event | category | flops | bytes accessed | tf_op | source)
XLA Modules:
  0.0 284.4 jit_solution(4137388919672703960)
XLA Ops:
  9.0 4.9 %collective-permute-start = (bf16[64,2]{0,1:T(2,128)(2,1)S(1)}, bf16[64,2]{0,1:T(2,128)(2,1)S(1)}, u32[]{:S(2)}, u32[]{:S(2)}) collective-permute-start(bf16[64,2]{0,1:T(2,128)(2,1)S(1)} %multiply_convert_fusion.1), channel_id=1, source_target_pairs={{0,16},{16,32},{32,48},{48,64},{64,80},{80,96},{96,112},{112,128},... | collective-permute-start | bytes 776 | tf_op jit(solution)/shard_map/ppermute | solution.py:107
  15.7 2.1 convolution_convert_fusion.1
  17.8 14.0 %all-to-all-start = ((bf16[16,2,32,128]{3,2,1,0:T(8,128)(2,1)}), bf16[16,2,32,128]{3,2,1,0:T(8,128)(2,1)S(1)}, u32[]{:S(2)}, u32[]{:S(2)}) async-start(bf16[16,2,32,128]{3,2,1,0:T(8,128)(2,1)} %bitcast.9), calls=%async_computation | async-start | bytes 524288 | tf_op jit(solution)/shard_map/all_to_all | solution.py:119
  34.4 14.3 %all-to-all-done = bf16[16,2,32,128]{3,2,1,0:T(8,128)(2,1)S(1)} async-done(((bf16[16,2,32,128]{3,2,1,0:T(8,128)(2,1)}), bf16[16,2,32,128]{3,2,1,0:T(8,128)(2,1)S(1)}, u32[]{:S(2)}, u32[]{:S(2)}) %all-to-all-start) | async-done | bytes 262176 | tf_op jit(solution)/shard_map/all_to_all | solution.py:119
  50.2 3.7 %collective-permute-start.1 = (bf16[512,128]{1,0:T(8,128)(2,1)S(1)}, bf16[512,128]{1,0:T(8,128)(2,1)S(1)}, u32[]{:S(2)}, u32[]{:S(2)}) collective-permute-start(bf16[512,128]{1,0:T(8,128)(2,1)S(1)} %bitcast.40), channel_id=1, source_target_pairs={{0,16},{16,0},{1,17},{17,1},{2,18},{18,2},{3,19},{19,3},{4,20},{20... | collective-permute-start | bytes 393224 | tf_op jit(solution)/shard_map/ppermute | solution.py:124
  54.9 1.7 broadcast_in_dim.8
  56.6 6.9 %all-to-all-start.1 = ((bf16[16,512,128]{2,1,0:T(8,128)(2,1)}), bf16[16,512,128]{2,1,0:T(8,128)(2,1)S(1)}, u32[]{:S(2)}, u32[]{:S(2)}) async-start(bf16[16,512,128]{2,1,0:T(8,128)(2,1)} %broadcast_in_dim.8), calls=%async_computation.1 | async-start | bytes 4194304 | tf_op jit(solution)/shard_map/all_to_all | solution.py:127
  63.5 1.6 slice.61
  65.1 33.5 %all-to-all-done.1.x_ref = bf16[16,512,128]{2,1,0:T(8,128)(2,1)S(1)} async-done(((bf16[16,512,128]{2,1,0:T(8,128)(2,1)}), bf16[16,512,128]{2,1,0:T(8,128)(2,1)S(1)}, u32[]{:S(2)}, u32[]{:S(2)}) %all-to-all-start.1) | async-done | bytes 2097184 | tf_op jit(solution)/shard_map/all_to_all | solution.py:127
  101.1 3.3 %shard_map.123 = bf16[16,512,128]{2,1,0:T(8,128)(2,1)} custom-call(bf16[16,512,128]{2,1,0:T(8,128)(2,1)S(1)} %all-to-all-done.1.x_ref, bf16[2048,256]{1,0:T(8,128)(2,1)S(1)} %bitcast.30, bf16[2048,256]{1,0:T(8,128)(2,1)S(1)} %bitcast.32, bf16[256,2048]{1,0:T(8,128)(2,1)S(1)} %bitcast.34), custom_call_target="tpu_custom_call" | custom-call | flops 1610612736 | bytes 7340032 | tf_op jit(solution)/shard_map/pallas_call | solution.py:33
  104.4 4.7 %all-to-all-start.2 = ((bf16[16,512,128]{2,1,0:T(8,128)(2,1)}), bf16[16,512,128]{2,1,0:T(8,128)(2,1)}, u32[]{:S(2)}, u32[]{:S(2)}) async-start(bf16[16,512,128]{2,1,0:T(8,128)(2,1)} %shard_map.123), calls=%async_computation.2 | async-start | bytes 4194304 | tf_op jit(solution)/shard_map/all_to_all | solution.py:136
  109.9 23.7 %all-gather.8.cloned.1.call-done.x_ref = bf16[16,512,128]{2,1,0:T(8,128)(2,1)} async-done(((bf16[1,512,128]{2,1,0:T(8,128)(2,1)}), bf16[16,512,128]{2,1,0:T(8,128)(2,1)}) %all-gather.8.cloned.1.call-update) | async-done | bytes 2097168 | tf_op jit(solution)/shard_map/all_gather | solution.py:126
  133.5 1.6 copy-done.6
  135.1 3.3 %shard_map.122 = bf16[16,512,128]{2,1,0:T(8,128)(2,1)} custom-call(bf16[16,512,128]{2,1,0:T(8,128)(2,1)S(1)} %copy-done.6, bf16[2048,256]{1,0:T(8,128)(2,1)S(1)} %bitcast.31, bf16[2048,256]{1,0:T(8,128)(2,1)S(1)} %bitcast.33, bf16[256,2048]{1,0:T(8,128)(2,1)S(1)} %bitcast.35), custom_call_target="tpu_custom_call" | custom-call | flops 1610612736 | bytes 7340032 | tf_op jit(solution)/shard_map/pallas_call | solution.py:33
  138.5 8.4 %all-to-all-done.2 = bf16[16,512,128]{2,1,0:T(8,128)(2,1)} async-done(((bf16[16,512,128]{2,1,0:T(8,128)(2,1)}), bf16[16,512,128]{2,1,0:T(8,128)(2,1)}, u32[]{:S(2)}, u32[]{:S(2)}) %all-to-all-start.2) | async-done | bytes 2097184 | tf_op jit(solution)/shard_map/all_to_all | solution.py:136
  146.9 3.7 %all-to-all-start.3 = ((bf16[16,512,128]{2,1,0:T(8,128)(2,1)}), bf16[16,512,128]{2,1,0:T(8,128)(2,1)S(1)}, u32[]{:S(2)}, u32[]{:S(2)}) async-start(bf16[16,512,128]{2,1,0:T(8,128)(2,1)} %shard_map.122), calls=%async_computation.3 | async-start | bytes 4194304 | tf_op jit(solution)/shard_map/all_to_all | solution.py:139
  150.6 1.9 reduce_sum.51
  152.5 2.9 %collective-permute-start.2 = (bf16[512,128]{1,0:T(8,128)(2,1)S(1)}, bf16[512,128]{1,0:T(8,128)(2,1)S(1)}, u32[]{:S(2)}, u32[]{:S(2)}) collective-permute-start(bf16[512,128]{1,0:T(8,128)(2,1)S(1)} %reduce_sum.51), channel_id=1, source_target_pairs={{0,16},{16,0},{1,17},{17,1},{2,18},{18,2},{3,19},{19,3},{4,20},{20... | collective-permute-start | bytes 393224 | tf_op jit(solution)/shard_map/ppermute | solution.py:140
  155.4 28.1 %all-to-all-done.3 = bf16[16,512,128]{2,1,0:T(8,128)(2,1)S(1)} async-done(((bf16[16,512,128]{2,1,0:T(8,128)(2,1)}), bf16[16,512,128]{2,1,0:T(8,128)(2,1)S(1)}, u32[]{:S(2)}, u32[]{:S(2)}) %all-to-all-start.3) | async-done | bytes 2097184 | tf_op jit(solution)/shard_map/all_to_all | solution.py:139
  184.5 10.1 %all-to-all-start.4 = ((bf16[16,2,32,128]{3,2,1,0:T(8,128)(2,1)}), bf16[16,2,32,128]{3,2,1,0:T(8,128)(2,1)S(1)}, u32[]{:S(2)}, u32[]{:S(2)}) async-start(bf16[16,2,32,128]{3,2,1,0:T(8,128)(2,1)} %pad_maximum_fusion.1), calls=%async_computation.4 | async-start | bytes 524288 | tf_op jit(solution)/shard_map/all_to_all | solution.py:149
  194.6 16.0 %all-gather.4.cloned.1.call-done = bf16[1024,1024]{1,0:T(8,128)(2,1)} async-done(((bf16[64,1024]{1,0:T(8,128)(2,1)}), bf16[1024,1024]{1,0:T(8,128)(2,1)}) %all-gather.4.cloned.1.call-update) | async-done | bytes 2097168 | tf_op jit(solution)/shard_map/all_gather | solution.py:116
  210.6 2.3 convolution_convert_fusion.2
  212.9 60.4 %all-gather.6.cloned.1.call-done = bf16[1024,1024]{1,0:T(8,128)(2,1)} async-done(((bf16[64,1024]{1,0:T(8,128)(2,1)}), bf16[1024,1024]{1,0:T(8,128)(2,1)}) %all-gather.6.cloned.1.call-update) | async-done | bytes 2097168 | tf_op jit(solution)/shard_map/all_gather | solution.py:131
  273.4 2.3 convolution_convert_fusion
  (51 shorter events, 14.9 us)
Async XLA Ops:
  7.2 203.4 %copy-start = (bf16[1024,128]{1,0:T(8,128)(2,1)S(1)}, bf16[1024,128]{1,0:T(8,128)(2,1)}, u32[]{:S(2)}) copy-start(bf16[1024,128]{1,0:T(8,128)(2,1)} %param.15) | copy-start | bytes 786436
  7.2 26.9 %copy-start.8 = (bf16[64,2048]{1,0:T(8,128)(2,1)S(1)}, bf16[64,2048]{1,0:T(8,128)(2,1)}, u32[]{:S(2)}) copy-start(bf16[64,2048]{1,0:T(8,128)(2,1)} %param.12) | copy-start | bytes 786436
  9.0 24.7 %collective-permute-start = (bf16[64,2]{0,1:T(2,128)(2,1)S(1)}, bf16[64,2]{0,1:T(2,128)(2,1)S(1)}, u32[]{:S(2)}, u32[]{:S(2)}) collective-permute-start(bf16[64,2]{0,1:T(2,128)(2,1)S(1)} %multiply_convert_fusion.1), channel_id=1, source_target_pairs={{0,16},{16,32},{32,48},{48,64},{64,80},{80,96},{96,112},{112,128},... | collective-permute-start | bytes 776 | tf_op jit(solution)/shard_map/ppermute | solution.py:107
  17.8 30.9 %all-to-all-start = ((bf16[16,2,32,128]{3,2,1,0:T(8,128)(2,1)}), bf16[16,2,32,128]{3,2,1,0:T(8,128)(2,1)S(1)}, u32[]{:S(2)}, u32[]{:S(2)}) async-start(bf16[16,2,32,128]{3,2,1,0:T(8,128)(2,1)} %bitcast.9), calls=%async_computation | async-start | bytes 524288 | tf_op jit(solution)/shard_map/all_to_all | solution.py:119
  31.9 101.7 %all-gather.8.cloned.1.call-start = ((), (), s32[]{:S(2)}) async-start(), calls=%async_computation.7 | async-start | bytes 2228224 | tf_op jit(solution)/shard_map/all_gather | solution.py:126
  34.4 20.5 %copy-start.7 = (bf16[64,2048]{1,0:T(8,128)(2,1)}, bf16[64,2048]{1,0:T(8,128)(2,1)S(1)}, u32[]{:S(2)}) copy-start(bf16[64,2048]{1,0:T(8,128)(2,1)S(1)} %fusion.6) | copy-start | bytes 786436
  49.5 161.1 %all-gather.4.cloned.1.call-start = ((), (), s32[]{:S(2)}) async-start(), calls=%async_computation.5 | async-start | bytes 2228224 | tf_op jit(solution)/shard_map/all_gather | solution.py:116
  50.2 4.7 %collective-permute-start.1 = (bf16[512,128]{1,0:T(8,128)(2,1)S(1)}, bf16[512,128]{1,0:T(8,128)(2,1)S(1)}, u32[]{:S(2)}, u32[]{:S(2)}) collective-permute-start(bf16[512,128]{1,0:T(8,128)(2,1)S(1)} %bitcast.40), channel_id=1, source_target_pairs={{0,16},{16,0},{1,17},{17,1},{2,18},{18,2},{3,19},{19,3},{4,20},{20... | collective-permute-start | bytes 393224 | tf_op jit(solution)/shard_map/ppermute | solution.py:124
  56.6 42.0 %copy-start.1 = (bf16[1,2048,256]{2,1,0:T(8,128)(2,1)S(1)}, bf16[1,2048,256]{2,1,0:T(8,128)(2,1)}, u32[]{:S(2)}) copy-start(bf16[1,2048,256]{2,1,0:T(8,128)(2,1)} %param.19) | copy-start | bytes 3145732
  56.6 42.0 %all-to-all-start.1 = ((bf16[16,512,128]{2,1,0:T(8,128)(2,1)}), bf16[16,512,128]{2,1,0:T(8,128)(2,1)S(1)}, u32[]{:S(2)}, u32[]{:S(2)}) async-start(bf16[16,512,128]{2,1,0:T(8,128)(2,1)} %broadcast_in_dim.8), calls=%async_computation.1 | async-start | bytes 4194304 | tf_op jit(solution)/shard_map/all_to_all | solution.py:127
  98.6 1.2 copy-start.2
  99.9 1.2 copy-start.4
  104.4 29.1 %copy-start.3 = (bf16[1,2048,256]{2,1,0:T(8,128)(2,1)S(1)}, bf16[1,2048,256]{2,1,0:T(8,128)(2,1)}, u32[]{:S(2)}) copy-start(bf16[1,2048,256]{2,1,0:T(8,128)(2,1)} %param.20) | copy-start | bytes 3145732
  104.4 29.1 %copy-start.5 = (bf16[1,256,2048]{2,1,0:T(8,128)(2,1)S(1)}, bf16[1,256,2048]{2,1,0:T(8,128)(2,1)}, u32[]{:S(2)}) copy-start(bf16[1,256,2048]{2,1,0:T(8,128)(2,1)} %param.21) | copy-start | bytes 3145732
  104.4 42.5 %all-to-all-start.2 = ((bf16[16,512,128]{2,1,0:T(8,128)(2,1)}), bf16[16,512,128]{2,1,0:T(8,128)(2,1)}, u32[]{:S(2)}, u32[]{:S(2)}) async-start(bf16[16,512,128]{2,1,0:T(8,128)(2,1)} %shard_map.123), calls=%async_computation.2 | async-start | bytes 4194304 | tf_op jit(solution)/shard_map/all_to_all | solution.py:136
  109.1 164.2 %all-gather.6.cloned.1.call-start = ((), (), s32[]{:S(2)}) async-start(), calls=%async_computation.6 | async-start | bytes 2228224 | tf_op jit(solution)/shard_map/all_gather | solution.py:131
  133.5 1.6 copy-start.6
  146.9 36.6 %all-to-all-start.3 = ((bf16[16,512,128]{2,1,0:T(8,128)(2,1)}), bf16[16,512,128]{2,1,0:T(8,128)(2,1)S(1)}, u32[]{:S(2)}, u32[]{:S(2)}) async-start(bf16[16,512,128]{2,1,0:T(8,128)(2,1)} %shard_map.122), calls=%async_computation.3 | async-start | bytes 4194304 | tf_op jit(solution)/shard_map/all_to_all | solution.py:139
  152.5 42.1 %copy-start.9 = (f32[256,2]{0,1:T(2,128)S(1)}, f32[256,2]{0,1:T(2,128)}, u32[]{:S(2)}) copy-start(f32[256,2]{0,1:T(2,128)} %param.18) | copy-start | bytes 6148
  152.5 31.2 %collective-permute-start.2 = (bf16[512,128]{1,0:T(8,128)(2,1)S(1)}, bf16[512,128]{1,0:T(8,128)(2,1)S(1)}, u32[]{:S(2)}, u32[]{:S(2)}) collective-permute-start(bf16[512,128]{1,0:T(8,128)(2,1)S(1)} %reduce_sum.51), channel_id=1, source_target_pairs={{0,16},{16,0},{1,17},{17,1},{2,18},{18,2},{3,19},{19,3},{4,20},{20... | collective-permute-start | bytes 393224 | tf_op jit(solution)/shard_map/ppermute | solution.py:140
  184.5 92.0 %all-to-all-start.4 = ((bf16[16,2,32,128]{3,2,1,0:T(8,128)(2,1)}), bf16[16,2,32,128]{3,2,1,0:T(8,128)(2,1)S(1)}, u32[]{:S(2)}, u32[]{:S(2)}) async-start(bf16[16,2,32,128]{3,2,1,0:T(8,128)(2,1)} %pad_maximum_fusion.1), calls=%async_computation.4 | async-start | bytes 524288 | tf_op jit(solution)/shard_map/all_to_all | solution.py:149
Sparse Core Ops, SparseCore 0:
  49.6 83.8 all-gather.7
  136.5 73.9 all-gather.3
  213.6 59.6 all-gather.5
